TPU v7x, 256 devices: a whole 4x4x8 slice. The times are simulated.
256 devices in a mesh: fs: 32 (over z, x), tp: 8 (over y, core).
Axes of the slice: x: 4, y: 4, z: 8, core: 2. Of those that a mesh axis runs over, the one named last changes fastest.
Arguments:
- saved_input: bfloat16 [81920, 2048], P('fs'), may hold values from -6 to 6
- value_cot: bfloat16 [81920, 1024], P('fs', 'tp'), may hold values from -6 to 6
- query_cot: bfloat16 [81920, 512], P('fs', 'tp'), may hold values from -6 to 6
- value_master: float32 [2048, 1024], P('fs', 'tp'), may hold values from -0.125 to 0.125
- query_master: float32 [2048, 512], P('fs', 'tp'), may hold values from -0.125 to 0.125
- value_factor: bfloat16 [2048, 256], P('fs'), may hold values from -0.125 to 0.125
- query_factor: bfloat16 [2048, 256], P('fs'), may hold values from -0.125 to 0.125
- value_first: float32 [256, 1024], P('fs', 'tp'), as said below
- value_second: float32 [256, 1024], P('fs', 'tp'), as said below
- query_first: float32 [256, 512], P('fs', 'tp'), as said below
- query_second: float32 [256, 512], P('fs', 'tp'), as said below
Outputs:
- value_step: float32 [2048, 1024], P('fs', 'tp')
- query_step: float32 [2048, 512], P('fs', 'tp')
- value_master_new: float32 [2048, 1024], P('fs', 'tp')
- query_master_new: float32 [2048, 512], P('fs', 'tp')
- value_copy: bfloat16 [2048, 1024], P(None, 'tp')
- query_copy: bfloat16 [2048, 512], P(None, 'tp')
- value_first_new: float32 [256, 1024], P('fs', 'tp')
- value_second_new: float32 [256, 1024], P('fs', 'tp')
- query_first_new: float32 [256, 512], P('fs', 'tp')
- query_second_new: float32 [256, 512], P('fs', 'tp')
Inputs may be any that keep to these rules, and one draw needn't show every extreme that they name: `value_first`: first moments are real-valued of the projected gradient's order. `value_second`: second moments are positive. `query_first`: first moments are real-valued of the projected gradient's order. `query_second`: second moments are positive.
All inputs are finite; a program needn't handle non-finite values.
Results may differ from a plain program's by a relative error of at most 0.001.
Values may be sent and summed in bfloat16 or wider, within the bound.
A program may use at most 64 MiB of HBM per device.

v0:
```python
import jax
import jax.numpy as jnp
from jax import lax
from jax.sharding import Mesh
from jax.sharding import PartitionSpec as P

RANK = 256
V_W = 1024
QK_W = 512
FS = ("fs_0", "fs_1")
FS_TP = ("fs_0", "fs_1", "tp_0", "tp_1")
TP = ("tp_0", "tp_1")


BETA_ONE = 0.9
BETA_TWO = 0.95
DENOM_EPS = 1e-08
NORM_EPS = 1e-06
STEP_SIZE = 0.05


def split_up(x, dim, size):
    dims = x.shape
    blocks = x.reshape(*dims[:dim], size, dims[dim] // size, *dims[dim + 1 :])
    return jnp.moveaxis(blocks, dim, 0)


def sent_and_summed(x, axis, dim):
    blocks = split_up(x, dim, lax.axis_size(axis))
    arrived = lax.all_to_all(blocks, axis, split_axis=0, concat_axis=0, tiled=True)
    return arrived.sum(axis=0)


def sent_together(arrays, axis, dim, along):
    ends, at = ([], 0)
    for a in arrays[:-1]:
        at += a.shape[along]
        ends.append(at)
    both = jnp.concatenate(arrays, axis=along)
    return tuple(jnp.split(sent_and_summed(both, axis, dim), ends, axis=along))


def sent_together_2(arrays, axis, dim, along):
    both = jnp.concatenate(arrays, axis=along)
    out, at, outs = (lax.all_gather(both, axis, axis=dim, tiled=True), 0, [])
    for a in arrays:
        outs.append(lax.slice_in_dim(out, at, at + a.shape[along], axis=along))
        at += a.shape[along]
    return tuple(outs)


def by_axis(x, axes):
    for axis in axes:
        x = lax.psum(x, axis)
    return x


def moment_update(projected, first, second):
    first_new = BETA_ONE * first + (1.0 - BETA_ONE) * projected
    second_new = BETA_TWO * second + (1.0 - BETA_TWO) * projected * projected
    direction = first_new / (jnp.sqrt(second_new) + DENOM_EPS)
    return (first_new, second_new, direction)


def token_product(left, right):
    return lax.dot_general(
        left, right, (((0,), (0,)), ((), ())), preferred_element_type=jnp.float32
    )


def on_device(
    saved_input,
    value_cot,
    query_cot,
    value_master,
    query_master,
    value_factor,
    query_factor,
    value_first,
    value_second,
    query_first,
    query_second,
):
    shards = lax.axis_size(FS)
    tokens_all = saved_input.shape[0] * shards
    highest = lax.Precision.HIGHEST
    columns = saved_input
    value_grad = sent_and_summed(token_product(columns, value_cot), FS, 0) / tokens_all
    columns = saved_input
    query_grad = sent_and_summed(token_product(columns, query_cot), FS, 0) / tokens_all
    value_part = jnp.dot(value_factor.astype(jnp.float32).T, value_grad, precision=highest)
    query_part = jnp.dot(query_factor.astype(jnp.float32).T, query_grad, precision=highest)
    value_share, query_share = sent_together((value_part, query_part), FS, 0, 1)
    value_first_new, value_second_new, value_dir_own = moment_update(
        value_share, value_first, value_second
    )
    query_first_new, query_second_new, query_dir_own = moment_update(
        query_share, query_first, query_second
    )
    value_direction, query_direction = sent_together_2((value_dir_own, query_dir_own), FS, 0, 1)
    square_sum = by_axis(
        jnp.sum(value_dir_own * value_dir_own) + jnp.sum(query_dir_own * query_dir_own), FS_TP
    )
    update_scale = 1.0 / jnp.sqrt(square_sum / (RANK * (V_W + QK_W)) + NORM_EPS)
    value_step = (
        jnp.dot(value_factor.astype(jnp.float32), value_direction, precision=highest) * update_scale
    )
    query_step = (
        jnp.dot(query_factor.astype(jnp.float32), query_direction, precision=highest) * update_scale
    )
    value_master_new = value_master - STEP_SIZE * value_step
    query_master_new = query_master - STEP_SIZE * query_step
    value_copy, query_copy = sent_together_2(
        (value_master_new.astype(jnp.bfloat16), query_master_new.astype(jnp.bfloat16)), FS, 0, 1
    )
    return (
        value_step,
        query_step,
        value_master_new,
        query_master_new,
        value_copy,
        query_copy,
        value_first_new,
        value_second_new,
        query_first_new,
        query_second_new,
    )


def solution(mesh):
    split = Mesh(mesh.devices.reshape(8, 4, 4, 2), ("fs_0", "fs_1", "tp_0", "tp_1"))
    placed = (
        P(FS, None),
        P(FS, TP),
        P(FS, TP),
        P(FS, TP),
        P(FS, TP),
        P(FS, None),
        P(FS, None),
        P(FS, TP),
        P(FS, TP),
        P(FS, TP),
        P(FS, TP),
    )
    return jax.shard_map(
        on_device,
        mesh=split,
        in_specs=placed,
        out_specs=(
            P(FS, TP),
            P(FS, TP),
            P(FS, TP),
            P(FS, TP),
            P(None, TP),
            P(None, TP),
            P(FS, TP),
            P(FS, TP),
            P(FS, TP),
            P(FS, TP),
        ),
        check_vma=False,
    )
```

profile of v0, /device:TPU:2, one launch (start us, length us, event | category | flops | bytes accessed | tf_op | source)
XLA Modules:
  0.0 230.8 jit_solution(3035166584856945840)
XLA Ops:
  0.6 0.0 copy-start
  0.7 6.1 %fusion.17 = f32[2048,64]{0,1:T(8,128)S(1)} fusion(bf16[2560,64]{0,1:T(8,128)(2,1)} %param.13, bf16[2560,2048]{1,0:T(8,128)(2,1)} %param.11), kind=kOutput, calls=%fused_computation.34 | convolution fusion | flops 671088640 | bytes 11337728 | tf_op jit(solution)/shard_map/dot_general | solution.py:66
  6.7 0.4 reshape.30
  7.2 0.6 copy.30
  7.8 0.0 copy-start.1
  7.8 1.4 reshape.32
  9.2 0.0 copy-start.2
  9.2 11.7 %all-to-all-start.1 = ((f32[32,1,4096]{2,1,0:T(1,128)}), f32[32,1,4096]{2,1,0:T(1,128)S(1)}, u32[]{:S(2)}, u32[]{:S(2)}) async-start(f32[32,1,4096]{2,1,0:T(1,128)} %reshape.32), calls=%async_computation.1 | async-start | bytes 1048576 | tf_op jit(solution)/shard_map/all_to_all | solution.py:30
  21.0 0.0 copy-done
  21.0 0.0 copy-start.5
  21.0 0.0 copy-start.6
  21.0 0.0 copy-start.7
  21.0 0.0 copy-start.8
  21.1 0.0 copy-start.3
  21.1 0.0 copy-start.4
  21.1 7.9 %fusion.16 = f32[2048,128]{1,0:T(8,128)} fusion(bf16[2560,2048]{1,0:T(8,128)(2,1)} %param.11, bf16[2560,128]{1,0:T(8,128)(2,1)S(1)} %copy-done), kind=kOutput, calls=%fused_computation.33 | convolution fusion | flops 1342177280 | bytes 12189696 | tf_op jit(solution)/shard_map/dot_general | solution.py:66
  29.0 8.8 %all-to-all-done.1 = f32[32,1,4096]{2,1,0:T(1,128)S(1)} async-done(((f32[32,1,4096]{2,1,0:T(1,128)}), f32[32,1,4096]{2,1,0:T(1,128)S(1)}, u32[]{:S(2)}, u32[]{:S(2)}) %all-to-all-start.1) | async-done | bytes 524320 | tf_op jit(solution)/shard_map/all_to_all | solution.py:30
  37.8 5.6 %all-to-all-start = ((f32[32,64,128]{2,1,0:T(8,128)}), f32[32,64,128]{2,1,0:T(8,128)S(1)}, u32[]{:S(2)}, u32[]{:S(2)}) async-start(f32[32,64,128]{2,1,0:T(8,128)} %bitcast), calls=%async_computation | async-start | bytes 2097152 | tf_op jit(solution)/shard_map/all_to_all | solution.py:30
  43.4 0.5 broadcast.6
  43.9 1.9 reduce
  45.8 0.4 reshape.33
  46.2 0.1 bitcast_reduce_fusion
  46.3 0.0 copy-done.1
  46.3 0.2 convolution_bitcast_fusion.1
  46.5 24.1 %all-to-all-done = f32[32,64,128]{2,1,0:T(8,128)S(1)} async-done(((f32[32,64,128]{2,1,0:T(8,128)}), f32[32,64,128]{2,1,0:T(8,128)S(1)}, u32[]{:S(2)}, u32[]{:S(2)}) %all-to-all-start) | async-done | bytes 1048608 | tf_op jit(solution)/shard_map/all_to_all | solution.py:30
  70.6 0.1 reduce_sum.45
  70.7 0.0 copy-done.2
  70.7 0.3 convolution_bitcast_fusion
  71.0 0.1 copy.26
  71.1 15.3 %all_to_all.15 = f32[32,8,192]{2,1,0:T(8,128)S(1)} all-to-all(f32[32,8,192]{2,1,0:T(8,128)S(1)} %bitcast.26), channel_id=1, replica_groups=mesh['fs_0'=8,'fs_1'=4,'tp_0'=4,'tp_1'=2] {'fs_0','fs_1'}, dimensions={0} | all-to-all | bytes 393216 | tf_op jit(solution)/shard_map/all_to_all | solution.py:30
  86.5 0.0 copy-done.5
  86.5 0.0 copy-done.6
  86.5 1.2 multiply_reduce_fusion
  87.7 0.0 copy-done.7
  87.7 0.0 copy-done.8
  87.7 1.2 multiply_reduce_fusion.1
  90.2 16.0 %psum.28 = f32[]{:T(128)} all-reduce(f32[]{:T(128)S(6)} %add.46), channel_id=1, replica_groups=mesh['fs_0'=8,'fs_1'=4,'tp_0'=4,'tp_1'=2] {'fs_0'}, use_global_device_ids=true, to_apply=%region_5.0 | all-reduce | flops 1 | bytes 8 | tf_op jit(solution)/shard_map/psum | solution.py:54
  106.2 10.0 %psum.29 = f32[]{:T(128)} all-reduce(f32[]{:T(128)} %psum.28), channel_id=1, replica_groups=mesh['fs_0'=8,'fs_1'=4,'tp_0'=4,'tp_1'=2] {'fs_1'}, use_global_device_ids=true, to_apply=%region_6.0 | all-reduce | flops 1 | bytes 8 | tf_op jit(solution)/shard_map/psum | solution.py:54
  116.2 11.3 %psum.30 = f32[]{:T(128)} all-reduce(f32[]{:T(128)} %psum.29), channel_id=1, replica_groups=mesh['fs_0'=8,'fs_1'=4,'tp_0'=4,'tp_1'=2] {'tp_0'}, use_global_device_ids=true, to_apply=%region_7.0 | all-reduce | flops 1 | bytes 8 | tf_op jit(solution)/shard_map/psum | solution.py:54
  127.5 47.2 %all_gather.6 = f32[256,192]{1,0:T(8,128)S(1)} all-gather(f32[8,192]{1,0:T(8,128)S(1)} %pad_maximum_fusion.2), channel_id=1, replica_groups=mesh['fs_0'=8,'fs_1'=4,'tp_0'=4,'tp_1'=2] {'fs_0','fs_1'}, dimensions={0}, use_global_device_ids=true | all-gather | bytes 202752 | tf_op jit(solution)/shard_map/all_gather | solution.py:45
  174.8 3.1 %psum.31 = f32[]{:T(128)} all-reduce(f32[]{:T(128)} %psum.30), channel_id=1, replica_groups=mesh['fs_0'=8,'fs_1'=4,'tp_0'=4,'tp_1'=2] {'tp_1'}, use_global_device_ids=true, to_apply=%region_8.0 | all-reduce | flops 1 | bytes 8 | tf_op jit(solution)/shard_map/psum | solution.py:54
  178.5 0.0 copy-done.3
  178.6 0.8 fusion.13
  179.4 0.0 copy-done.4
  179.4 0.8 fusion.12
  180.2 48.9 %all_gather.7 = bf16[2048,192]{1,0:T(8,128)(2,1)S(1)} all-gather(bf16[64,192]{1,0:T(8,128)(2,1)S(1)} %pad_maximum_fusion.1), channel_id=1, replica_groups=mesh['fs_0'=8,'fs_1'=4,'tp_0'=4,'tp_1'=2] {'fs_0','fs_1'}, dimensions={0}, use_global_device_ids=true | all-gather | bytes 811008 | tf_op jit(solution)/shard_map/all_gather | solution.py:45
  229.1 0.8 slice.18
  229.9 0.9 copy.27
  (5 shorter events, 0.1 us)
Async XLA Ops:
  0.6 20.4 %copy-start = (bf16[2560,128]{1,0:T(8,128)(2,1)S(1)}, bf16[2560,128]{1,0:T(8,128)(2,1)}, u32[]{:S(2)}) copy-start(bf16[2560,128]{1,0:T(8,128)(2,1)} %param.12) | copy-start | bytes 1966084
  7.8 38.5 %copy-start.1 = (bf16[64,256]{1,0:T(8,128)(2,1)S(1)}, bf16[64,256]{1,0:T(8,128)(2,1)}, u32[]{:S(2)}) copy-start(bf16[64,256]{1,0:T(8,128)(2,1)} %param.17) | copy-start | bytes 98308
  9.2 61.4 %copy-start.2 = (bf16[64,256]{1,0:T(8,128)(2,1)S(1)}, bf16[64,256]{1,0:T(8,128)(2,1)}, u32[]{:S(2)}) copy-start(bf16[64,256]{1,0:T(8,128)(2,1)} %param.16) | copy-start | bytes 98308
  9.2 28.6 %all-to-all-start.1 = ((f32[32,1,4096]{2,1,0:T(1,128)}), f32[32,1,4096]{2,1,0:T(1,128)S(1)}, u32[]{:S(2)}, u32[]{:S(2)}) async-start(f32[32,1,4096]{2,1,0:T(1,128)} %reshape.32), calls=%async_computation.1 | async-start | bytes 1048576 | tf_op jit(solution)/shard_map/all_to_all | solution.py:30
  21.0 65.5 %copy-start.5 = (f32[8,64]{1,0:T(8,128)S(1)}, f32[8,64]{1,0:T(8,128)}, u32[]{:S(2)}) copy-start(f32[8,64]{1,0:T(8,128)} %param.21) | copy-start | bytes 6148
  21.0 65.4 %copy-start.6 = (f32[8,64]{1,0:T(8,128)S(1)}, f32[8,64]{1,0:T(8,128)}, u32[]{:S(2)}) copy-start(f32[8,64]{1,0:T(8,128)} %param.20) | copy-start | bytes 6148
  21.0 66.6 %copy-start.7 = (f32[8,128]{1,0:T(8,128)S(1)}, f32[8,128]{1,0:T(8,128)}, u32[]{:S(2)}) copy-start(f32[8,128]{1,0:T(8,128)} %param.19) | copy-start | bytes 12292
  21.0 66.6 %copy-start.8 = (f32[8,128]{1,0:T(8,128)S(1)}, f32[8,128]{1,0:T(8,128)}, u32[]{:S(2)}) copy-start(f32[8,128]{1,0:T(8,128)} %param.18) | copy-start | bytes 12292
  21.1 157.5 %copy-start.3 = (f32[64,64]{1,0:T(8,128)S(1)}, f32[64,64]{1,0:T(8,128)}, u32[]{:S(2)}) copy-start(f32[64,64]{1,0:T(8,128)} %param.15) | copy-start | bytes 49156
  21.1 158.3 %copy-start.4 = (f32[64,128]{1,0:T(8,128)S(1)}, f32[64,128]{1,0:T(8,128)}, u32[]{:S(2)}) copy-start(f32[64,128]{1,0:T(8,128)} %param.14) | copy-start | bytes 98308
  37.8 32.8 %all-to-all-start = ((f32[32,64,128]{2,1,0:T(8,128)}), f32[32,64,128]{2,1,0:T(8,128)S(1)}, u32[]{:S(2)}, u32[]{:S(2)}) async-start(f32[32,64,128]{2,1,0:T(8,128)} %bitcast), calls=%async_computation | async-start | bytes 2097152 | tf_op jit(solution)/shard_map/all_to_all | solution.py:30
where the time goes:
time: 231 us
  blocking collectives  152 us (66%)
  waiting for transfers between devices  32.9 us (14%)
  starting transfers between devices  17.3 us (7%)
  matrix products  16.1 us (7%)
  local copies, waits for them, and re-layouts  5.34 us (2%)
  other arithmetic  4.52 us (2%)
  between operations  2.85 us (1%)
    all_gather x2, blocking collectives, sent_together_2(): out, at, outs = (lax.all_gather(both, axis, axis=dim, tiled=True), 0, [])  96.1 us
    psum x4, blocking collectives, by_axis(): x = lax.psum(x, axis)  40.4 us
    all_to_all x2, waiting for transfers between devices, sent_and_summed(): lax.all_to_all(blocks, axis, split_axis=0, concat_axis=0, tiled=True)  32.9 us
    all_to_all x2, starting transfers between devices, sent_and_summed(): lax.all_to_all(blocks, axis, split_axis=0, concat_axis=0, tiled=True)  17.3 us
    all_to_all x1, blocking collectives, sent_and_summed(): lax.all_to_all(blocks, axis, split_axis=0, concat_axis=0, tiled=True)  15.3 us
    dot_general x2, matrix products, token_product(): lax.dot_general(left, right, (((0,), (0,)), ((), ())), preferred_element_...  14 us
  transfers between devices with their start and end apart: 2, of which 2 were waited for; matrix products, arithmetic and copies ran while one was open for 5% of the time, Pallas kernels for 0%

commit v1 on v0

v1 whole, which is shorter than its diff:
```python
import jax
import jax.numpy as jnp
from jax import lax
from jax.experimental import pallas as pl
from jax.experimental.pallas import tpu as pltpu
from jax.sharding import Mesh
from jax.sharding import PartitionSpec as P

FS = ("z", "x")
TP = ("y", "c")
TOKENS = 81920
BETA_ONE = 0.9
BETA_TWO = 0.95
DENOM_EPS = 1e-08
NORM_EPS = 1e-06
STEP_SIZE = 0.05
ENTRIES = 256 * (1024 + 512)
NZ, NX, NY, NC = 8, 4, 4, 2
SHARDS = NZ * NX
MESH = pl.DeviceIdType.MESH
BLOCKS = 8
BLOCK = 256
F32, BF16 = jnp.float32, jnp.bfloat16


def mod(a, n):
    return lax.rem(a, n)


def ring_distance(d, n):
    return min(d, n - d)


OFFSETS = sorted(
    [(dz, dx) for dz in range(NZ) for dx in range(NX) if dz or dx],
    key=lambda o: -(ring_distance(o[0], NZ) + ring_distance(o[1], NX)),
)


def arrived(ref, sem):
    pltpu.make_async_copy(ref, ref, sem).wait()


def send(src, dst, ssem, rsem, to):
    pltpu.make_async_remote_copy(
        src_ref=src, dst_ref=dst, send_sem=ssem, recv_sem=rsem, device_id=to, device_id_type=MESH
    ).start()


class Gather:
    def __init__(self, buf, recv, sent, z, x, forward=None):
        self.buf, self.recv, self.sent, self.z, self.x, self.forward = buf, recv, sent, z, x, forward

    def at(self, dz, dx):
        owner = mod(self.z + NZ - dz, NZ) * NX + mod(self.x + NX - dx, NX)
        return self.buf.at[owner]

    def put(self, dz, dx, sz, sx):
        block = self.at(dz, dx)
        to = {}
        if sz:
            to["z"] = mod(self.z + NZ + sz, NZ)
        if sx:
            to["x"] = mod(self.x + NX + sx, NX)
        place = ((dz + sz) % NZ) * NX + (dx + sx) % NX
        send(block, block, self.sent, self.recv.at[place], to)

    def take(self, dz, dx):
        block = self.at(dz, dx)
        arrived(block, self.recv.at[dz * NX + dx])
        if self.forward is not None:
            self.forward(block)

    def sent_all(self):
        part = self.buf.at[pl.ds(0, SHARDS - 1)]
        arrived(part, self.sent)


class XThenZ(Gather):
    UP = (4, 4, 3, 3)

    def step(self, s):
        if s == 0:
            for dx in (2, 1, 3):
                self.put(0, 0, 0, dx)
            self.put(0, 0, 1, 0)
            self.put(0, 0, -1, 0)
        elif s == 1:
            for dx in (1, 3, 2):
                self.take(0, dx)
                self.put(0, dx, 1, 0)
                self.put(0, dx, -1, 0)
        else:
            k = s - 1
            for dx in (0, 1, 3, 2):
                up, down = self.UP[dx], 7 - self.UP[dx]
                if k <= up:
                    self.take(k, dx)
                    if k < up:
                        self.put(k, dx, 1, 0)
                if k <= down:
                    self.take(NZ - k, dx)
                    if k < down:
                        self.put(NZ - k, dx, -1, 0)


class ZThenX(Gather):
    WAVES = ((1, 7), (2, 6), (3, 5), (4,))

    def step(self, s):
        if s == 0:
            for dz in (4, 3, 5, 2, 6, 1, 7):
                self.put(0, 0, dz, 0)
            for dx in (2, 1, 3):
                self.put(0, 0, 0, dx)
        elif s <= 4:
            for dz in self.WAVES[s - 1]:
                self.take(dz, 0)
                for dx in (2, 1, 3):
                    self.put(dz, 0, 0, dx)
        else:
            for dz in (0, 1, 7, 2, 6, 3, 5, 4):
                for dx in (1, 3, 2):
                    self.take(dz, dx)


def halves(a):
    hi = a.astype(BF16)
    return hi, (a - hi.astype(F32)).astype(BF16)


def moments(projected, first, second):
    first_new = BETA_ONE * first + (1.0 - BETA_ONE) * projected
    second_new = BETA_TWO * second + (1.0 - BETA_TWO) * projected * projected
    return first_new, second_new, first_new / (jnp.sqrt(second_new) + DENOM_EPS)


def dot(a, b):
    return jnp.dot(a, b, preferred_element_type=F32)


def kernel(
    x_hbm, cv_hbm, cq_hbm, mv_hbm, mq_hbm, fv_hbm, fq_hbm, v1_hbm, v2_hbm, q1_hbm, q2_hbm,
    step_v, step_q, new_v, new_q, copy_v, copy_q, v1_new, v2_new, q1_new, q2_new,
    xb, cv, ct, lv, lq, pv, pq, mb, mq, m1v, m2v, m1q, m2q,
    part, got, dirs, dv, dq, sv, sq, squares,
    in_sem, x_sem, p_recv, m_recv, p_sent, m_sent, d_sent, d_recv, b_sent, b_recv, c_sent, c_recv, s_sent, s_recv,
):
    z, x, y, c = (lax.axis_index(a) for a in ("z", "x", "y", "c"))
    me = z * NX + x
    tp = y * NC + c

    def load(src, dst, i):
        copy = pltpu.make_async_copy(src, dst, in_sem.at[i])
        copy.start()
        return copy

    loads = [
        load(fv_hbm, pv.at[me], 0),
        load(fq_hbm, pq.at[me], 1),
        load(cv_hbm, cv, 2),
        load(cq_hbm, ct.at[pl.ds(128, 64)], 3),
    ]
    x_loads = [
        pltpu.make_async_copy(x_hbm.at[:, pl.ds(BLOCK * j, BLOCK)], xb.at[j], x_sem.at[j]) for j in range(BLOCKS)
    ]
    for copy in x_loads:
        copy.start()
    loads += [
        load(mv_hbm, mb.at[me, pl.ds(0, 64)], 4),
        load(mq_hbm, mq, 5),
        load(v1_hbm, m1v, 6),
        load(v2_hbm, m2v, 7),
        load(q1_hbm, m1q, 8),
        load(q2_hbm, m2q, 9),
    ]

    barrier = pltpu.get_barrier_semaphore()
    greeted = 0
    for dx in range(1, NX):
        pl.semaphore_signal(barrier, inc=1, device_id={"x": mod(x + dx, NX)}, device_id_type=MESH)
        greeted += 1
    for dz in range(1, NZ):
        pl.semaphore_signal(barrier, inc=1, device_id={"z": mod(z + dz, NZ)}, device_id_type=MESH)
        greeted += 1
    tp_peers = []
    for dy in range(NY):
        for dc in range(NC):
            if dy or dc:
                tp_peers.append({"y": mod(y + dy, NY), "c": mod(c + dc, NC)})
    for peer in tp_peers:
        pl.semaphore_signal(barrier, inc=1, device_id=peer, device_id_type=MESH)
        greeted += 1

    partner = {"c": 1 - c}

    def to_partner(block):
        send(block, block, d_sent, d_recv, partner)

    first, second = c == 0, c == 1
    p_x = XThenZ(pv, p_recv, p_sent, z, x, to_partner)
    p_z = ZThenX(pq, p_recv, p_sent, z, x, to_partner)
    m_x = XThenZ(mb, m_recv, m_sent, z, x)
    m_z = ZThenX(mb, m_recv, m_sent, z, x)

    def p_step(*steps):
        @pl.when(first)
        def _():
            for s in steps:
                p_x.step(s)

        @pl.when(second)
        def _():
            for s in steps:
                p_z.step(s)

    def m_step(*steps):
        @pl.when(first)
        def _():
            for s in steps:
                m_z.step(s)

        @pl.when(second)
        def _():
            for s in steps:
                m_x.step(s)

    loads[2].wait()
    loads[3].wait()

    def turn(i, _):
        rows = pl.ds(pl.multiple_of(i * 256, 256), 256)
        ct[pl.ds(0, 128), rows] = cv[rows, :].T
        return ()

    lax.fori_loop(0, 10, turn, ())

    def product(j, _):
        pltpu.make_async_copy(x_hbm.at[:, pl.ds(0, BLOCK)], xb.at[j], x_sem.at[j]).wait()
        g = dot(ct[...], xb[j])
        hi, lo = halves(g)
        lv[j, pl.ds(0, 128), :] = hi[:128]
        lv[j, pl.ds(128, 128), :] = lo[:128]
        lq[j, pl.ds(0, 64), :] = hi[128:]
        lq[j, pl.ds(64, 64), :] = lo[128:]
        return ()

    lax.fori_loop(0, 4, product, ())
    loads[0].wait()
    loads[1].wait()
    pl.semaphore_wait(barrier, greeted)
    p_step(0)
    lax.fori_loop(4, BLOCKS, product, ())
    for copy in loads[4:]:
        copy.wait()
    mb[me, pl.ds(64, 32), :] = jnp.concatenate([mq[pl.ds(0, 32), :], mq[pl.ds(32, 32), :]], axis=1)
    p_step(1, 2, 3)
    p_step(4, 5)
    m_step(0)

    @pl.when(first)
    def _():
        arrived(pq.at[pl.ds(0, SHARDS - 1)], d_recv)

    @pl.when(second)
    def _():
        arrived(pv.at[pl.ds(0, SHARDS - 1)], d_recv)

    def project(j, total):
        tv, tq = total
        slab = pl.ds(pl.multiple_of(4 * j, 4), 4)
        return tv + dot(lv[j], pv[slab].reshape(BLOCK, 256)), tq + dot(lq[j], pq[slab].reshape(BLOCK, 256))

    tv, tq = lax.fori_loop(0, BLOCKS, project, (jnp.zeros((256, 256), F32), jnp.zeros((128, 256), F32)))
    own_v = (tv[:128] + tv[128:]).T
    own_q = tq[:64] + tq[64:]
    own_q = jnp.concatenate([own_q, own_q], axis=0).T
    low = lax.broadcasted_iota(jnp.int32, (4, 128), 1) < 64
    for f in range(SHARDS):
        part[f, 0] = own_v[8 * f : 8 * f + 4]
        part[f, 1] = own_v[8 * f + 4 : 8 * f + 8]
        part[f, 2] = jnp.where(low, own_q[8 * f : 8 * f + 4], own_q[8 * f + 4 : 8 * f + 8])

    for dz, dx in OFFSETS:
        to_z, to_x = mod(z + dz, NZ), mod(x + dx, NX)
        send(part.at[to_z * NX + to_x], got.at[dz * NX + dx - 1], b_sent, b_recv, {"z": to_z, "x": to_x})
    m_step(1)
    arrived(got, b_recv)
    total = (jnp.sum(got[...], axis=0) + part[me]) * (1.0 / TOKENS)
    proj_v = jnp.concatenate([total[0], total[1]], axis=0)
    proj_q = total[2]

    def packed(ref):
        return jnp.concatenate([ref[pl.ds(0, 4), :], ref[pl.ds(4, 4), :]], axis=1)

    a_v, b_v, d_v = moments(proj_v, m1v[...], m2v[...])
    a_q, b_q, d_q = moments(proj_q, packed(m1q), packed(m2q))
    dirs[me, 0] = d_v[:4]
    dirs[me, 1] = d_v[4:]
    dirs[me, 2] = d_q
    v1_new[...] = a_v
    v2_new[...] = b_v
    for ref, val in ((q1_new, a_q), (q2_new, b_q)):
        ref[pl.ds(0, 4), :] = val[:, :64]
        ref[pl.ds(4, 4), :] = val[:, 64:]
    for dz, dx in OFFSETS:
        to_z, to_x = mod(z + dz, NZ), mod(x + dx, NX)
        send(dirs.at[me], dirs.at[me], c_sent, c_recv, {"z": to_z, "x": to_x})
    m_step(2, 3)
    arrived(dirs.at[pl.ds(0, SHARDS - 1)], c_recv)

    all_dirs = dirs[...]
    squares[tp] = jnp.sum(all_dirs * all_dirs, axis=(0, 1))
    for peer in tp_peers:
        send(squares.at[tp], squares.at[tp], s_sent, s_recv, peer)

    for f in range(SHARDS):
        dv[pl.ds(8 * f, 4), :] = dirs[f, 0]
        dv[pl.ds(8 * f + 4, 4), :] = dirs[f, 1]
        dq[pl.ds(8 * f, 4), :] = dirs[f, 2]
        dq[pl.ds(8 * f + 4, 4), :] = pltpu.roll(dirs[f, 2], 64, 1)
    right_v = jnp.concatenate(halves(dv[...]), axis=1)
    right_q = jnp.concatenate(halves(dq[...]), axis=1)

    def steps(j, _):
        slab = pl.ds(pl.multiple_of(4 * j, 4), 4)
        s = dot(pv[slab].reshape(BLOCK, 256), right_v)
        sv[j] = s[:, :128] + s[:, 128:]
        s = dot(pq[slab].reshape(BLOCK, 256), right_q)
        sq[j] = s[:, :128] + s[:, 128:]
        return ()

    lax.fori_loop(0, BLOCKS, steps, ())
    m_step(4, 5)
    arrived(squares.at[pl.ds(0, 7)], s_recv)
    square_sum = jnp.sum(jnp.sum(squares[...], axis=0), keepdims=True)
    scale = 1.0 / jnp.sqrt(square_sum / ENTRIES + NORM_EPS)

    def finish(j, _):
        for i in range(4):
            rows = pl.ds(pl.multiple_of(256 * j + 64 * i, 64), 64)
            master = mb[4 * j + i, pl.ds(0, 64), :]
            copy_v[rows, :] = (master - STEP_SIZE * (sv[j, pl.ds(64 * i, 64), :] * scale)).astype(BF16)
        for i in range(2):
            pair = []
            for k in range(2):
                m = mb[4 * j + 2 * i + k, pl.ds(64, 32), :]
                pair += [m, pltpu.roll(m, 64, 1)]
            master = jnp.concatenate(pair, axis=0)
            new = master - STEP_SIZE * (sq[j, pl.ds(128 * i, 128), :] * scale)
            columns = pl.ds(pl.multiple_of(256 * j + 128 * i, 128), 128)
            copy_q[:, columns] = new.T[:64].astype(BF16)
        return ()

    lax.fori_loop(0, BLOCKS, finish, ())
    mine = pl.ds(pl.multiple_of(64 * x, 64), 64)
    own = sv[z, mine, :] * scale
    step_v[...] = own
    new_v[...] = mb[me, pl.ds(0, 64), :] - STEP_SIZE * own
    own = (sq[z, mine, :] * scale)[:, :64]
    step_q[...] = own
    new_q[...] = mq[...] - STEP_SIZE * own

    p_x.sent_all()
    m_x.sent_all()
    arrived(pv.at[pl.ds(0, SHARDS - 1)], d_sent)
    arrived(got, b_sent)
    arrived(got, c_sent)
    arrived(squares.at[pl.ds(0, 7)], s_sent)


def on_device(
    saved_input, value_cot, query_cot, value_master, query_master, value_factor, query_factor,
    value_first, value_second, query_first, query_second,
):
    vmem = pltpu.VMEM
    dma = pltpu.SemaphoreType.DMA
    shape = jax.ShapeDtypeStruct
    out = pl.pallas_call(
        kernel,
        out_shape=(
            shape((64, 128), F32),
            shape((64, 64), F32),
            shape((64, 128), F32),
            shape((64, 64), F32),
            shape((2048, 128), BF16),
            shape((64, 2048), BF16),
            shape((8, 128), F32),
            shape((8, 128), F32),
            shape((8, 64), F32),
            shape((8, 64), F32),
        ),
        in_specs=[pl.BlockSpec(memory_space=pl.ANY)] * 11,
        out_specs=tuple([pl.BlockSpec(memory_space=pltpu.VMEM)] * 10),
        scratch_shapes=[
            vmem((BLOCKS, 2560, BLOCK), BF16),
            vmem((2560, 128), BF16),
            vmem((192, 2560), BF16),
            vmem((BLOCKS, 256, BLOCK), BF16),
            vmem((BLOCKS, 128, BLOCK), BF16),
            vmem((SHARDS, 64, 256), BF16),
            vmem((SHARDS, 64, 256), BF16),
            vmem((SHARDS, 96, 128), F32),
            vmem((64, 64), F32),
            vmem((8, 128), F32),
            vmem((8, 128), F32),
            vmem((8, 64), F32),
            vmem((8, 64), F32),
            vmem((SHARDS, 3, 4, 128), F32),
            vmem((SHARDS - 1, 3, 4, 128), F32),
            vmem((SHARDS, 3, 4, 128), F32),
            vmem((256, 128), F32),
            vmem((256, 128), F32),
            vmem((BLOCKS, BLOCK, 128), F32),
            vmem((BLOCKS, BLOCK, 128), F32),
            vmem((8, 4, 128), F32),
            dma((10,)),
            dma((BLOCKS,)),
            dma((SHARDS,)),
            dma((SHARDS,)),
            dma,
            dma,
            dma,
            dma,
            dma,
            dma,
            dma,
            dma,
            dma,
            dma,
        ],
        compiler_params=pltpu.CompilerParams(collective_id=0, has_side_effects=True),
        name="moment_update",
    )(
        saved_input, value_cot, query_cot.T, value_master, query_master, value_factor, query_factor,
        value_first, value_second, query_first, query_second,
    )
    step_v, step_q, new_v, new_q, copy_v, copy_q, v1, v2, q1, q2 = out
    return step_v, step_q, new_v, new_q, copy_v, copy_q.T, v1, v2, q1, q2


def solution(mesh):
    split = Mesh(mesh.devices.reshape(NZ, NX, NY, NC), ("z", "x", "y", "c"))
    both = P(FS, TP)
    return jax.shard_map(
        on_device,
        mesh=split,
        in_specs=(P(FS, None), both, both, both, both, P(FS, None), P(FS, None), both, both, both, both),
        out_specs=(both, both, both, both, P(None, TP), P(None, TP), both, both, both, both),
        check_vma=False,
    )
```

time: 231 us -> 72.7 us (0.31)
  blocking collectives: 152 us -> 0 us
  Pallas kernels: 0 us -> 56.5 us
  waiting for transfers between devices: 32.9 us -> 0 us
  starting transfers between devices: 17.3 us -> 0 us
  matrix products: 16.1 us -> 0 us
  local copies, waits for them, and re-layouts: 5.34 us -> 14.1 us
  other arithmetic: 4.52 us -> 0 us
    all_gather x2 -> x0, blocking collectives: 96.1 us -> none  [sent_together_2(): out, at, outs = (lax.all_gather(both, axis, axis=dim, tiled=True), 0, [])]
    pallas_call x0 -> x1, Pallas kernels: none -> 56.5 us  [on_device(): pl.pallas_call(kernel, out_shape=(shape((64, 128), F32), shape((64, 64),...]
    psum x4 -> x0, blocking collectives: 40.4 us -> none  [by_axis(): x = lax.psum(x, axis)]
    all_to_all x2 -> x0, waiting for transfers between devices: 32.9 us -> none  [sent_and_summed(): lax.all_to_all(blocks, axis, split_axis=0, concat_axis=0, tiled=True)]
    all_to_all x2 -> x0, starting transfers between devices: 17.3 us -> none  [sent_and_summed(): lax.all_to_all(blocks, axis, split_axis=0, concat_axis=0, tiled=True)]
    dot_general x6 -> x0, matrix products: 16.1 us -> none  [the longest x2 14 us: token_product(): lax.dot_general(left, right, (((0,), (0,)), ((), ())), preferred_element_...]
    all_to_all x1 -> x0, blocking collectives: 15.3 us -> none  [sent_and_summed(): lax.all_to_all(blocks, axis, split_axis=0, concat_axis=0, tiled=True)]
    unnamed x21 -> x10, local copies, waits for them, and re-layouts: 2.81 us -> 14.1 us
  transfers between devices with their start and end apart: 2 -> 0, of which waited for: 2 -> 0; matrix products, arithmetic and copies ran while one was open for 5% -> 0% of each run, Pallas kernels for 0% -> 0%
where the time goes in v1:
time: 72.7 us; the launch traced here: 71.3 us
  Pallas kernels  56.5 us (78%)
  local copies, waits for them, and re-layouts  14.1 us (19%)
    pallas_call x1, Pallas kernels, on_device(): pl.pallas_call(kernel, out_shape=(shape((64, 128), F32), shape((64, 64),...  56.5 us
    unnamed x10, local copies, waits for them, and re-layouts  14.1 us

profile of v1, /device:TPU:2, one launch (start us, length us, event | category | flops | bytes accessed | tf_op | source)
XLA Modules:
  0.0 71.3 jit_solution(15784373092467530630)
XLA Ops:
  0.6 56.5 %moment_update.1 = (f32[64,128]{1,0:T(8,128)}, f32[64,64]{1,0:T(8,128)}, f32[64,128]{1,0:T(8,128)}, f32[64,64]{1,0:T(8,128)}, bf16[2048,128]{1,0:T(8,128)(2,1)},...) custom-call(bf16[2560,2048]{1,0:T(8,128)(2,1)} %x_hbm.1, ...), custom_call_target="tpu_custom_call" | custom-call | tf_op jit(solution)/shard_map/moment_update/pallas_call | solution.py:379
  57.2 1.4 %copy.31 = f32[64,128]{1,0:T(8,128)} copy(f32[64,128]{1,0:T(8,128)} %get-tuple-element.40) | data formatting | bytes 65536
  58.5 1.4 %copy.32 = f32[64,64]{1,0:T(8,128)} copy(f32[64,64]{1,0:T(8,128)} %get-tuple-element.41) | data formatting | bytes 32768
  59.9 1.4 %copy.33 = f32[64,128]{1,0:T(8,128)} copy(f32[64,128]{1,0:T(8,128)} %get-tuple-element.42) | data formatting | bytes 65536
  61.3 1.4 %copy.34 = f32[64,64]{1,0:T(8,128)} copy(f32[64,64]{1,0:T(8,128)} %get-tuple-element.43) | data formatting | bytes 32768
  62.7 1.9 %copy.35 = bf16[2048,128]{1,0:T(8,128)(2,1)} copy(bf16[2048,128]{1,0:T(8,128)(2,1)} %get-tuple-element.44) | data formatting | bytes 1048576
  64.5 1.7 %copy.36 = bf16[2048,64]{0,1:T(8,128)(2,1)} copy(bf16[2048,64]{0,1:T(8,128)(2,1)} %bitcast.3) | data formatting | bytes 524288
  66.2 1.3 %copy.37 = f32[8,128]{1,0:T(8,128)} copy(f32[8,128]{1,0:T(8,128)} %get-tuple-element.46) | data formatting | bytes 8192
  67.5 1.3 %copy.38 = f32[8,128]{1,0:T(8,128)} copy(f32[8,128]{1,0:T(8,128)} %get-tuple-element.47) | data formatting | bytes 8192
  68.7 1.3 %copy.39 = f32[8,64]{1,0:T(8,128)} copy(f32[8,64]{1,0:T(8,128)} %get-tuple-element.48) | data formatting | bytes 4096
  70.0 1.3 %copy.40 = f32[8,64]{1,0:T(8,128)} copy(f32[8,64]{1,0:T(8,128)} %get-tuple-element.49) | data formatting | bytes 4096
